TPU v7x, 32 devices: a whole 2x2x4 slice. The times are simulated.
32 devices in a mesh: tp: 8 (over z, y), dp: 4 (over x, core).
Axes of the slice: x: 2, y: 2, z: 4, core: 2. Of those that a mesh axis runs over, the one named last changes fastest.
Arguments:
- tokens: bfloat16 [64, 4096], P('tp', 'dp'), may hold values from -30 to 30
- lengths: int32 [64], P('dp'), may hold values from 1 to 2048, 16384 in all
- states: float32 [2, 64, 2048, 128], P(None, 'dp', 'tp'), may hold values from -0.8 to 0.8
- norm_gain: bfloat16 [2, 4096], P(None, 'dp'), may hold values from 0.099609375 to 1.8984375
- w_query: bfloat16 [2, 4096, 2048], P(None, 'dp', 'tp'), may hold values from -0.09375 to 0.09375
- w_key: bfloat16 [2, 4096, 2048], P(None, 'dp', 'tp'), may hold values from -0.09375 to 0.09375
- w_value: bfloat16 [2, 4096, 2048], P(None, 'dp', 'tp'), may hold values from -0.09375 to 0.09375
- w_gate: bfloat16 [2, 4096, 2048], P(None, 'dp', 'tp'), may hold values from -0.09375 to 0.09375
- head_gain: bfloat16 [2, 2048], P(None, 'tp'), may hold values from 0.099609375 to 1.8984375
- w_out: bfloat16 [2, 2048, 4096], P(None, 'tp', 'dp'), may hold values from -0.125 to 0.125
Outputs:
- hidden_out: bfloat16 [64, 4096], P('tp', 'dp')
- new_states: float32 [2, 64, 2048, 128], P(None, 'dp', 'tp')
All inputs are finite; a program needn't handle non-finite values. No bound on the sum of `lengths` on one device may be relied on, other than what follows from the above.
Results may differ from a plain program's by a relative error of at most 0.012.
Values may be sent and summed in bfloat16 or wider, within the bound.
A program may use at most 64 MiB of HBM per device.

v0:
```python
import functools
import math

import jax
import jax.numpy as jnp
from jax import lax
from jax.experimental import pallas as pl
from jax.experimental.pallas import tpu as pltpu
from jax.sharding import PartitionSpec as P

D = 4096
HEADS = 16
DK = 128
LAYERS = 2


norm_eps = 1e-06
group_eps = 1e-05
rotary_base = 10000.0


def partner_2(value, axis, apart):
    mask = 2**apart
    pairs = [(source, source ^ mask) for source in range(lax.axis_size(axis))]
    return lax.ppermute(value, axis, pairs)


def rotate(values, positions):
    half_size = values.shape[-1] // 2
    inverse = rotary_base ** (-jnp.arange(half_size, dtype=jnp.float32) / half_size)
    angles = positions.astype(jnp.float32)[:, None] * inverse[None, :]
    cosine = jnp.cos(angles)[:, None, :]
    sine_v = jnp.sin(angles)[:, None, :]
    first_part = values[..., :half_size]
    second = values[..., half_size:]
    return jnp.concatenate(
        [first_part * cosine - second * sine_v, first_part * sine_v + second * cosine], axis=-1
    )


def decays(head_ids):
    return 1.0 - jnp.exp2(-1.0 - 9.0 * head_ids.astype(jnp.float32) / (HEADS - 1))


def split_head_body(tokens, lengths, states, norm_gain, w_query, w_key, w_value, w_gate, head_gain, w_out):
    tp_index = lax.axis_index("tp")
    dp_index = lax.axis_index("dp")
    tp_count = lax.axis_size("tp")
    columns = w_query.shape[2]
    pieces = max(DK // columns, 1)
    levels = pieces.bit_length() - 1
    local_heads = max(columns // DK, 1)
    value_cols = columns // local_heads
    head_ids = tp_index * columns // DK + jnp.arange(local_heads, dtype=jnp.int32)
    gammas = decays(head_ids)
    hidden_x = tokens
    outputs = []
    for layer_id in range(LAYERS):
        prior_state = states[layer_id]
        row_total = prior_state.shape[0]
        local_rows = hidden_x.shape[0]
        x_float = hidden_x.astype(jnp.float32)
        feature_gain = norm_gain[layer_id].astype(jnp.float32)
        weights = jnp.concatenate(
            [w_query[layer_id], w_key[layer_id], w_value[layer_id], w_gate[layer_id]], axis=1
        )
        gathered = lax.all_gather(hidden_x, "tp", axis=0, tiled=True)
        gathered_f = gathered.astype(jnp.float32)
        normed = (gathered_f * feature_gain).astype(jnp.bfloat16)
        partial_value = jnp.dot(normed, weights, preferred_element_type=jnp.float32)
        squares_full = jnp.zeros((local_rows * tp_count,), jnp.float32)
        squares_full = lax.dynamic_update_slice_in_dim(
            squares_full, jnp.sum(x_float * x_float, axis=1), tp_index * local_rows, 0
        )
        all_squares = lax.psum(squares_full, ("tp", "dp"))
        summed = lax.psum_scatter(partial_value, "dp", scatter_dimension=0, tiled=True)
        own_squares = lax.dynamic_slice_in_dim(all_squares, dp_index * row_total, row_total, 0)
        row_scale = lax.rsqrt(own_squares / D + norm_eps)
        projected = (summed * row_scale[:, None]).astype(jnp.bfloat16)
        query_rows = projected[:, :columns]
        key_rows = projected[:, columns : 2 * columns]
        value_rows = projected[:, 2 * columns : 3 * columns]
        gate_rows = projected[:, 3 * columns :]
        stacked = jnp.stack([query_rows, key_rows])
        for join_level_id in range(levels):
            partner = partner_2(stacked, "tp", join_level_id)
            upper_bit = tp_index // 2**join_level_id % 2
            stacked = jnp.where(
                upper_bit == 1,
                jnp.concatenate([partner, stacked], axis=-1),
                jnp.concatenate([stacked, partner], axis=-1),
            )
        query_f = rotate(
            stacked[0].astype(jnp.float32).reshape(row_total, local_heads, DK), lengths
        )
        key_f = rotate(
            stacked[1].astype(jnp.float32).reshape(row_total, local_heads, DK), lengths
        ) * DK ** (-0.5)
        values_f = value_rows.astype(jnp.float32).reshape(row_total, local_heads, value_cols)
        state_view = prior_state.reshape(row_total, local_heads, value_cols, DK)
        updated = gammas[None, :, None, None] * state_view + jnp.einsum(
            "shd,shv->shvd", key_f, values_f
        )
        readout = jnp.einsum("shd,shvd->shv", query_f, updated)
        head_stats = jnp.stack([jnp.sum(readout, axis=-1), jnp.sum(readout * readout, axis=-1)])
        for level_id in range(levels):
            head_stats = head_stats + partner_2(head_stats, "tp", level_id)
        mean_v = head_stats[0][..., None] / DK
        square = head_stats[1][..., None] / DK
        grouped = ((readout - mean_v) * lax.rsqrt(square - mean_v * mean_v + group_eps)).reshape(
            row_total, columns
        )
        grouped = grouped * head_gain[layer_id].astype(jnp.float32)
        gated_rows = (jax.nn.silu(gate_rows.astype(jnp.float32)) * grouped).astype(jnp.bfloat16)
        out_weight = w_out[layer_id]
        whole_weight = lax.all_gather(out_weight, "tp", axis=0, tiled=True)
        every_row = lax.all_gather(gated_rows, "dp", axis=0, tiled=True)
        owned_rows = lax.all_to_all(every_row, "tp", split_axis=0, concat_axis=1, tiled=True)
        branch = jnp.dot(owned_rows, whole_weight, preferred_element_type=jnp.float32)
        hidden_x, updated = (
            (x_float + branch).astype(jnp.bfloat16),
            updated.reshape(row_total, columns, DK),
        )
        outputs.append(updated)
    return (hidden_x, jnp.stack(outputs))


MESH = pl.DeviceIdType.MESH
KINDS = 4
OUT_PIECES = 4


def decay_row(columns):
    channel = lax.axis_index("tp") * columns + lax.broadcasted_iota(jnp.int32, (1, columns), 1)
    head = (channel // DK).astype(jnp.float32)
    return 1.0 - jnp.exp((-1.0 - 9.0 * head / (HEADS - 1)) * math.log(2.0))


def step_kernel(
    tokens,
    lengths,
    norm_gain,
    head_gain,
    states,
    w_query,
    w_key,
    w_value,
    w_gate,
    w_out,
    hidden,
    new_states,
    length_in,
    norm_in,
    head_in,
    state_in,
    state_t,
    w_in,
    w_back,
    gathered,
    part,
    part_in,
    sq,
    sq_in,
    gated,
    branch,
    branch_in,
    fresh,
    load_sem,
    x_send,
    x_recv,
    p_send,
    p_recv,
    q_send,
    q_recv,
    g_send,
    g_recv,
    b_send,
    b_recv,
):
    tp, dp = lax.axis_index("tp"), lax.axis_index("dp")
    tpn, dpn = lax.axis_size("tp"), lax.axis_size("dp")
    rows, features = tokens.shape
    seqs, columns = new_states.shape[1:3]
    heads = columns // DK
    total = rows * tpn

    barrier = pltpu.get_barrier_semaphore()
    tp_peers = [lax.rem(tp + o, tpn) for o in range(tpn)]
    dp_peers = [lax.rem(dp + o, dpn) for o in range(dpn)]
    for o in range(1, tpn):
        pl.semaphore_signal(barrier, inc=1, device_id=(tp_peers[o], dp), device_id_type=MESH)
    for o in range(1, dpn):
        pl.semaphore_signal(barrier, inc=1, device_id=(tp, dp_peers[o]), device_id_type=MESH)

    loads = []

    def load(src, dst):
        copy = pltpu.make_async_copy(src, dst, load_sem.at[len(loads)])
        copy.start()
        loads.append(copy)
        return copy

    got_x = load(tokens, gathered.at[0, tp])
    got_small = [load(lengths, length_in), load(norm_gain, norm_in), load(head_gain, head_in)]
    got_in, got_state, got_back = [], [], []
    for layer in range(LAYERS):
        got_in.append(
            [
                load(w.at[layer], w_in.at[layer, j])
                for j, w in enumerate((w_query, w_key, w_value, w_gate))
            ]
        )
        got_state.append(load(states.at[layer], state_in.at[layer]))
        got_back.append(load(w_out.at[layer], w_back.at[layer]))

    for copy in got_small:
        copy.wait()
    half = DK // 2
    lane = lax.broadcasted_iota(jnp.int32, (seqs, DK), 1)
    row = lax.broadcasted_iota(jnp.int32, (seqs, DK), 0)
    position = jnp.zeros((seqs, DK), jnp.float32)
    for s in range(seqs):
        position = jnp.where(row == s, length_in[s].astype(jnp.float32), position)
    inverse = jnp.exp((lane % half).astype(jnp.float32) * (-math.log(rotary_base) / half))
    angle = position * inverse
    cosine = jnp.cos(angle)
    sine = jnp.sin(angle)
    sine = jnp.where(lane < half, -sine, sine)
    gamma = decay_row(columns)

    def decay_of(h):
        return gamma[:, h * DK : h * DK + 1]

    pl.semaphore_wait(barrier, tpn + dpn - 2)

    def send(src, dst, send_sem, recv_sem, where):
        copy = pltpu.make_async_remote_copy(
            src_ref=src,
            dst_ref=dst,
            send_sem=send_sem,
            recv_sem=recv_sem,
            device_id=where,
            device_id_type=MESH,
        )
        copy.start()
        return copy

    def spread_x(layer, src):
        return [
            send(
                src,
                gathered.at[layer, tp],
                x_send.at[layer, o],
                x_recv.at[layer, o],
                (tp_peers[o], dp),
            )
            for o in sorted(range(1, tpn), key=lambda o: -min(o, tpn - o))
        ]

    def turn_state(layer):
        got_state[layer].wait()
        for s in range(seqs):
            block = jnp.transpose(state_in[layer, s])
            state_t[layer, s * DK : (s + 1) * DK] = (block * gamma).astype(jnp.bfloat16)

    sent = []
    got_x.wait()
    x_copies = spread_x(0, gathered.at[0, tp])
    x_own = gathered[0, pl.ds(tp, 1)][0].astype(jnp.float32)
    turn_state(0)
    for layer in range(LAYERS):
        for copy in x_copies:
            copy.wait_recv()
        sent += x_copies
        x_all = gathered[layer].astype(jnp.float32).reshape(total, features)
        normed = (x_all * norm_in[layer : layer + 1, :].astype(jnp.float32)).astype(jnp.bfloat16)
        part_copies = []
        for j in range(KINDS):
            got_in[layer][j].wait()
            product = jnp.dot(normed, w_in[layer, j], preferred_element_type=jnp.float32)
            part[layer, j] = product.astype(jnp.bfloat16).reshape(dpn, seqs, columns)
            part_copies.append(
                [
                    send(
                        part.at[layer, j, dp_peers[o]],
                        part_in.at[layer, j, o - 1],
                        p_send.at[layer, j, o],
                        p_recv.at[layer, j, o],
                        (tp, dp_peers[o]),
                    )
                    for o in range(1, dpn)
                ]
            )
            if j == 0:
                squares = jnp.sum(x_all * x_all, axis=1, keepdims=True)
                sq[layer] = jnp.broadcast_to(squares, (total, DK)).reshape(dpn, seqs, DK)
                sq_copies = [
                    send(
                        sq.at[layer, dp_peers[o]],
                        sq_in.at[layer, o - 1],
                        q_send.at[layer, o],
                        q_recv.at[layer, o],
                        (tp, dp_peers[o]),
                    )
                    for o in range(1, dpn)
                ]
        for copy in sq_copies:
            copy.wait_recv()
        sent += sq_copies
        own_squares = sq[layer, pl.ds(dp, 1)][0]
        for o in range(1, dpn):
            own_squares = own_squares + sq_in[layer, o - 1]
        row_scale = lax.rsqrt(own_squares[:, :1] / D + norm_eps)

        def project(j):
            for copy in part_copies[j]:
                copy.wait_recv()
            sent.extend(part_copies[j])
            summed = part[layer, j, pl.ds(dp, 1)][0].astype(jnp.float32)
            for o in range(1, dpn):
                summed = summed + part_in[layer, j, o - 1].astype(jnp.float32)
            return (summed * row_scale).astype(jnp.bfloat16).astype(jnp.float32)

        def rotated(rows_in, h):
            one = rows_in[:, h * DK : (h + 1) * DK]
            return one * cosine + pltpu.roll(one, half, 1) * sine

        query = project(0)
        queries = [rotated(query, h) for h in range(heads)]
        tall = jnp.concatenate(queries, axis=0)
        tall_row = lax.broadcasted_iota(jnp.int32, tall.shape, 0) % seqs
        wide = jnp.concatenate([jnp.where(tall_row == s, tall, 0.0) for s in range(seqs)], axis=1)
        read = jnp.dot(
            wide.astype(jnp.bfloat16), state_t[layer], preferred_element_type=jnp.float32
        )
        key = project(1)
        rotated_keys = [rotated(key, h) * DK ** (-0.5) for h in range(heads)]
        value = project(2)
        gate = project(3)
        silu = gate / (1.0 + jnp.exp(-gate))
        gains = head_in[layer : layer + 1, :].astype(jnp.float32)
        outs = []
        for h in range(heads):
            at = slice(h * DK, (h + 1) * DK)
            score = jnp.sum(queries[h] * rotated_keys[h], axis=1, keepdims=True)
            readout = read[h * seqs : (h + 1) * seqs, at] + score * value[:, at]
            mean = jnp.sum(readout, axis=1, keepdims=True) / DK
            square = jnp.sum(readout * readout, axis=1, keepdims=True) / DK
            grouped = (readout - mean) * lax.rsqrt(square - mean * mean + group_eps)
            outs.append(silu[:, at] * grouped * gains[:, at])
        gated[layer, pl.ds(dp, 1)] = jnp.concatenate(outs, axis=1).astype(jnp.bfloat16)[None]
        gated_copies = [
            send(
                gated.at[layer, dp],
                gated.at[layer, dp],
                g_send.at[layer, o],
                g_recv.at[layer, o],
                (tp, dp_peers[o]),
            )
            for o in range(1, dpn)
        ]
        turned = jnp.transpose(value)

        def advance(first, last):
            for s in range(first, last):
                for h in range(heads):
                    at = slice(h * DK, (h + 1) * DK)
                    new_states[layer, s, at] = (
                        decay_of(h) * state_in[layer, s, at]
                        + turned[at, s : s + 1] * rotated_keys[h][s : s + 1]
                    )

        advance(0, seqs // 4)
        got_back[layer].wait()
        for copy in gated_copies:
            copy.wait_recv()
        sent += gated_copies
        every = gated[layer].reshape(dpn * seqs, columns)
        product = jnp.dot(every, w_back[layer], preferred_element_type=jnp.float32)
        branch[layer] = product.reshape(tpn, rows, features).astype(jnp.bfloat16)
        branch_copies = [
            send(
                branch.at[layer, tp_peers[o]],
                branch_in.at[layer, o - 1],
                b_send.at[layer, o],
                b_recv.at[layer, o],
                (tp_peers[o], dp),
            )
            for o in range(1, tpn)
        ]
        advance(seqs // 4, seqs)
        if layer + 1 < LAYERS:
            turn_state(layer + 1)
        added = branch[layer, pl.ds(tp, 1)][0].astype(jnp.float32)
        for o in range(1, tpn):
            branch_copies[o - 1].wait_recv()
            added = added + branch_in[layer, o - 1].astype(jnp.float32)
        sent += branch_copies
        new_x = (x_own + added).astype(jnp.bfloat16)
        if layer + 1 < LAYERS:
            fresh[...] = new_x
            gathered[layer + 1, pl.ds(tp, 1)] = new_x[None]
            x_own = new_x.astype(jnp.float32)
            x_copies = spread_x(layer + 1, fresh)
        else:
            hidden[...] = new_x
    for copy in sent:
        copy.wait_send()


def deliver_kernel(hidden_in, states_in, hidden, states, sem):
    layers, seqs = states.shape[:2]
    pieces = math.gcd(seqs, OUT_PIECES)
    copies = [pltpu.make_async_copy(hidden_in, hidden, sem.at[0])]
    for piece in range(layers * pieces):
        at = (piece // pieces, pl.ds(piece % pieces * (seqs // pieces), seqs // pieces))
        copies.append(pltpu.make_async_copy(states_in.at[at], states.at[at], sem.at[piece + 1]))
    for copy in copies:
        copy.start()
    for copy in copies:
        copy.wait()


def body(tokens, lengths, states, norm_gain, w_query, w_key, w_value, w_gate, head_gain, w_out):
    columns = w_query.shape[2]
    if columns % DK:
        return split_head_body(
            tokens, lengths, states, norm_gain, w_query, w_key, w_value, w_gate, head_gain, w_out
        )
    tpn, dpn = lax.axis_size("tp"), lax.axis_size("dp")
    rows, features = tokens.shape
    seqs = lengths.shape[0]
    vmem = pl.BlockSpec(memory_space=pltpu.VMEM)
    away = pl.BlockSpec(memory_space=pltpu.HBM)
    dma = pltpu.SemaphoreType.DMA
    bf16, f32 = jnp.bfloat16, jnp.float32
    hidden, new_states = pl.pallas_call(
        step_kernel,
        out_shape=(
            pltpu.VMEM((rows, features), bf16),
            pltpu.VMEM(states.shape, f32),
        ),
        in_specs=[away] * 10,
        out_specs=(vmem, vmem),
        scratch_shapes=[
            pltpu.SMEM(lengths.shape, jnp.int32),
            pltpu.VMEM(norm_gain.shape, bf16),
            pltpu.VMEM(head_gain.shape, bf16),
            pltpu.VMEM((LAYERS, seqs, columns, DK), f32),
            pltpu.VMEM((LAYERS, seqs * DK, columns), bf16),
            pltpu.VMEM((LAYERS, KINDS, features, columns), bf16),
            pltpu.VMEM((LAYERS, columns, features), bf16),
            pltpu.VMEM((LAYERS, tpn, rows, features), bf16),
            pltpu.VMEM((LAYERS, KINDS, dpn, seqs, columns), bf16),
            pltpu.VMEM((LAYERS, KINDS, dpn - 1, seqs, columns), bf16),
            pltpu.VMEM((LAYERS, dpn, seqs, DK), f32),
            pltpu.VMEM((LAYERS, dpn - 1, seqs, DK), f32),
            pltpu.VMEM((LAYERS, dpn, seqs, columns), bf16),
            pltpu.VMEM((LAYERS, tpn, rows, features), bf16),
            pltpu.VMEM((LAYERS, tpn - 1, rows, features), bf16),
            pltpu.VMEM((rows, features), bf16),
            dma((LAYERS * (KINDS + 2) + 4,)),
            dma((LAYERS, tpn)),
            dma((LAYERS, tpn)),
            dma((LAYERS, KINDS, dpn)),
            dma((LAYERS, KINDS, dpn)),
            dma((LAYERS, dpn)),
            dma((LAYERS, dpn)),
            dma((LAYERS, dpn)),
            dma((LAYERS, dpn)),
            dma((LAYERS, tpn)),
            dma((LAYERS, tpn)),
        ],
        compiler_params=pltpu.CompilerParams(collective_id=0, has_side_effects=True, vmem_limit_bytes=40 * 1024 * 1024),
    )(
        *(
            pltpu.with_memory_space_constraint(a, pltpu.HBM)
            for a in (
                tokens,
                lengths,
                norm_gain,
                head_gain,
                states,
                w_query,
                w_key,
                w_value,
                w_gate,
                w_out,
            )
        )
    )
    return pl.pallas_call(
        deliver_kernel,
        out_shape=(
            jax.ShapeDtypeStruct((rows, features), bf16),
            jax.ShapeDtypeStruct(states.shape, f32),
        ),
        in_specs=[vmem, vmem],
        out_specs=(away, away),
        scratch_shapes=[dma((LAYERS * OUT_PIECES + 1,))],
        compiler_params=pltpu.CompilerParams(vmem_limit_bytes=8 * 1024 * 1024),
    )(hidden, new_states)


def solution(mesh):
    placed = (
        P("tp", "dp"),
        P("dp"),
        P(None, "dp", "tp", None),
        P(None, "dp"),
        P(None, "dp", "tp"),
        P(None, "dp", "tp"),
        P(None, "dp", "tp"),
        P(None, "dp", "tp"),
        P(None, "tp"),
        P(None, "tp", "dp"),
    )
    return jax.shard_map(
        body,
        mesh=mesh,
        in_specs=placed,
        out_specs=(P("tp", "dp"), P(None, "dp", "tp", None)),
        check_vma=False,
    )
```

profile of v0, /device:TPU:0, one launch (start us, length us, event | category | flops | bytes accessed | tf_op | source)
XLA Modules:
  0.0 43.0 jit_solution(12412261084265615865)
XLA Ops:
  0.6 40.2 %shard_map.113 = (bf16[8,1024]{1,0:T(8,128)(2,1)S(1)}, f32[2,16,256,128]{3,2,1,0:T(8,128)S(1)}) custom-call(bf16[8,1024]{1,0:T(8,128)(2,1)} %tokens.1, s32[16]{0:T(128)} %lengths.1, bf16[2,1024]{1,0:T(2,128)(2,1)} %norm_gain.1, bf16[2,256]{1,0:T(2,128)(2,1)} %head_gain.1, f32[2,16,256,128]{3,2,1,0:T(8,128)} %states.1, bf16[2,1024,256]{2,1,0:T(8,128)(2,1)} %w_query.1, ...), custom_call_target="tpu_custom_call" | custom-call | tf_op jit(solution)/shard_map/pallas_call | solution.py:437
  40.9 2.1 %shard_map.114 = (bf16[8,1024]{1,0:T(8,128)(2,1)}, f32[2,16,256,128]{3,2,1,0:T(8,128)}) custom-call(bf16[8,1024]{1,0:T(8,128)(2,1)S(1)} %get-tuple-element.4.hidden_in, f32[2,16,256,128]{3,2,1,0:T(8,128)S(1)} %get-tuple-element.5.states_in), custom_call_target="tpu_custom_call" | custom-call | tf_op jit(solution)/shard_map/pallas_call | solution.py:492
where the time goes:
time: 43.1 us; the launch traced here: 43 us
  Pallas kernels  42.3 us (98%)
  between operations  0.64 us (1%)
    pallas_call x1, Pallas kernels, body(): pl.pallas_call(step_kernel, out_shape=(pltpu.VMEM((rows, features), bf16)...  40.2 us
    pallas_call x1, Pallas kernels, body(): pl.pallas_call(deliver_kernel, out_shape=(jax.ShapeDtypeStruct((rows, fea...  2.09 us

commit v1 on v0

--- a/solution.py
+++ b/solution.py
@@ -1,4 +1,4 @@
-import functools
+import contextlib
 import math
 
 import jax
@@ -127,13 +127,37 @@
 
 MESH = pl.DeviceIdType.MESH
 KINDS = 4
+GROUP = 2
+GROUPS = KINDS // GROUP
 OUT_PIECES = 4
+TRACED = False
+
+
+def stage(name):
+    return jax.named_scope(name) if TRACED else contextlib.nullcontext()
 
 
 def decay_row(columns):
     channel = lax.axis_index("tp") * columns + lax.broadcasted_iota(jnp.int32, (1, columns), 1)
     head = (channel // DK).astype(jnp.float32)
     return 1.0 - jnp.exp((-1.0 - 9.0 * head / (HEADS - 1)) * math.log(2.0))
+
+
+def flipped(index, mask):
+    for bit in range(mask.bit_length()):
+        if mask >> bit & 1:
+            index = index + (1 - index // 2**bit % 2 * 2) * 2**bit
+    return index
+
+
+def peers_of(index, count):
+    if count & (count - 1):
+        return [lax.rem(index + o, count) for o in range(count)]
+    return [flipped(index, mask) for mask in range(count)]
+
+
+def await_bytes(ref, sem):
+    pltpu.make_async_copy(ref, ref, sem).wait()
 
 
 def step_kernel(
@@ -165,16 +189,15 @@
     branch,
     branch_in,
     fresh,
-    load_sem,
-    x_send,
+    small_sem,
+    w_sem,
+    state_sem,
+    back_sem,
+    send_sem,
     x_recv,
-    p_send,
     p_recv,
-    q_send,
     q_recv,
-    g_send,
     g_recv,
-    b_send,
     b_recv,
 ):
     tp, dp = lax.axis_index("tp"), lax.axis_index("dp")
@@ -185,36 +208,32 @@
     total = rows * tpn
 
     barrier = pltpu.get_barrier_semaphore()
-    tp_peers = [lax.rem(tp + o, tpn) for o in range(tpn)]
-    dp_peers = [lax.rem(dp + o, dpn) for o in range(dpn)]
+    tp_peers, dp_peers = peers_of(tp, tpn), peers_of(dp, dpn)
     for o in range(1, tpn):
         pl.semaphore_signal(barrier, inc=1, device_id=(tp_peers[o], dp), device_id_type=MESH)
     for o in range(1, dpn):
         pl.semaphore_signal(barrier, inc=1, device_id=(tp, dp_peers[o]), device_id_type=MESH)
 
-    loads = []
-
-    def load(src, dst):
-        copy = pltpu.make_async_copy(src, dst, load_sem.at[len(loads)])
+    def load(src, dst, sem):
+        copy = pltpu.make_async_copy(src, dst, sem)
         copy.start()
-        loads.append(copy)
         return copy
 
-    got_x = load(tokens, gathered.at[0, tp])
-    got_small = [load(lengths, length_in), load(norm_gain, norm_in), load(head_gain, head_in)]
-    got_in, got_state, got_back = [], [], []
+    got_x = load(tokens, gathered.at[tp], small_sem.at[0])
+    got_small = [
+        load(lengths, length_in, small_sem.at[1]),
+        load(norm_gain, norm_in, small_sem.at[2]),
+        load(head_gain, head_in, small_sem.at[3]),
+    ]
+    for copy in [got_x, *got_small]:
+        copy.wait()
+    got_state, got_back = [], []
     for layer in range(LAYERS):
-        got_in.append(
-            [
-                load(w.at[layer], w_in.at[layer, j])
-                for j, w in enumerate((w_query, w_key, w_value, w_gate))
-            ]
-        )
-        got_state.append(load(states.at[layer], state_in.at[layer]))
-        got_back.append(load(w_out.at[layer], w_back.at[layer]))
-
-    for copy in got_small:
-        copy.wait()
+        for j, w in enumerate((w_query, w_key, w_value, w_gate)):
+            load(w.at[layer], w_in.at[layer, j], w_sem.at[layer])
+        got_state.append(load(states.at[layer], state_in.at[layer], state_sem.at[layer]))
+        got_back.append(load(w_out.at[layer], w_back.at[layer], back_sem.at[layer]))
+
     half = DK // 2
     lane = lax.broadcasted_iota(jnp.int32, (seqs, DK), 1)
     row = lax.broadcasted_iota(jnp.int32, (seqs, DK), 0)
@@ -231,31 +250,24 @@
     def decay_of(h):
         return gamma[:, h * DK : h * DK + 1]
 
-    pl.semaphore_wait(barrier, tpn + dpn - 2)
-
-    def send(src, dst, send_sem, recv_sem, where):
-        copy = pltpu.make_async_remote_copy(
+    with stage("bar_wait"):
+        pl.semaphore_wait(barrier, tpn + dpn - 2)
+
+    def send(src, dst, kind, recv_sem, where):
+        pltpu.make_async_remote_copy(
             src_ref=src,
             dst_ref=dst,
-            send_sem=send_sem,
+            send_sem=send_sem.at[kind],
             recv_sem=recv_sem,
             device_id=where,
             device_id_type=MESH,
-        )
-        copy.start()
-        return copy
+        ).start()
+
+    tp_order = sorted(range(1, tpn), key=lambda o: (-o.bit_count(), -o))
 
     def spread_x(layer, src):
-        return [
-            send(
-                src,
-                gathered.at[layer, tp],
-                x_send.at[layer, o],
-                x_recv.at[layer, o],
-                (tp_peers[o], dp),
-            )
-            for o in sorted(range(1, tpn), key=lambda o: -min(o, tpn - o))
-        ]
+        for o in tp_order:
+            send(src, gathered.at[layer * tpn + tp], 0, x_recv.at[layer], (tp_peers[o], dp))
 
     def turn_state(layer):
         got_state[layer].wait()
@@ -263,106 +275,102 @@
             block = jnp.transpose(state_in[layer, s])
             state_t[layer, s * DK : (s + 1) * DK] = (block * gamma).astype(jnp.bfloat16)
 
-    sent = []
-    got_x.wait()
-    x_copies = spread_x(0, gathered.at[0, tp])
-    x_own = gathered[0, pl.ds(tp, 1)][0].astype(jnp.float32)
-    turn_state(0)
+    spread_x(0, gathered.at[tp])
+    x_own = gathered[pl.ds(tp, 1)][0].astype(jnp.float32)
+    with stage("turn0"):
+        turn_state(0)
     for layer in range(LAYERS):
-        for copy in x_copies:
-            copy.wait_recv()
-        sent += x_copies
-        x_all = gathered[layer].astype(jnp.float32).reshape(total, features)
-        normed = (x_all * norm_in[layer : layer + 1, :].astype(jnp.float32)).astype(jnp.bfloat16)
-        part_copies = []
-        for j in range(KINDS):
-            got_in[layer][j].wait()
-            product = jnp.dot(normed, w_in[layer, j], preferred_element_type=jnp.float32)
-            part[layer, j] = product.astype(jnp.bfloat16).reshape(dpn, seqs, columns)
-            part_copies.append(
-                [
+        first = layer * tpn
+        await_bytes(w_in.at[layer], w_sem.at[layer])
+        with stage(f"L{layer}_wait_x"):
+            await_bytes(gathered.at[pl.ds(first, tpn - 1)], x_recv.at[layer])
+        with stage(f"L{layer}_sq"):
+            x_all = gathered[first : first + tpn].astype(jnp.float32).reshape(total, features)
+            squares = x_all[:, :DK] * x_all[:, :DK]
+            for at in range(DK, features, DK):
+                squares = squares + x_all[:, at : at + DK] * x_all[:, at : at + DK]
+            sq[layer * dpn : (layer + 1) * dpn] = squares.reshape(dpn, seqs, DK)
+            for o in reversed(range(1, dpn)):
+                send(
+                    sq.at[layer * dpn + dp_peers[o]],
+                    sq_in.at[layer, o - 1],
+                    1,
+                    q_recv.at[layer],
+                    (tp, dp_peers[o]),
+                )
+            normed = (x_all * norm_in[layer : layer + 1, :].astype(jnp.float32)).astype(jnp.bfloat16)
+        for group in range(GROUPS):
+            slot = (layer * GROUPS + group) * dpn
+            with stage(f"L{layer}_dots{group}"):
+                for i in range(GROUP):
+                    product = jnp.dot(
+                        normed, w_in[layer, group * GROUP + i], preferred_element_type=jnp.float32
+                    )
+                    part[slot : slot + dpn, i] = product.astype(jnp.bfloat16).reshape(dpn, seqs, columns)
+                for o in reversed(range(1, dpn)):
                     send(
-                        part.at[layer, j, dp_peers[o]],
-                        part_in.at[layer, j, o - 1],
-                        p_send.at[layer, j, o],
-                        p_recv.at[layer, j, o],
+                        part.at[slot + dp_peers[o]],
+                        part_in.at[layer * GROUPS + group, o - 1],
+                        2,
+                        p_recv.at[layer * GROUPS + group],
                         (tp, dp_peers[o]),
                     )
-                    for o in range(1, dpn)
-                ]
-            )
-            if j == 0:
-                squares = jnp.sum(x_all * x_all, axis=1, keepdims=True)
-                sq[layer] = jnp.broadcast_to(squares, (total, DK)).reshape(dpn, seqs, DK)
-                sq_copies = [
-                    send(
-                        sq.at[layer, dp_peers[o]],
-                        sq_in.at[layer, o - 1],
-                        q_send.at[layer, o],
-                        q_recv.at[layer, o],
-                        (tp, dp_peers[o]),
-                    )
-                    for o in range(1, dpn)
-                ]
-        for copy in sq_copies:
-            copy.wait_recv()
-        sent += sq_copies
-        own_squares = sq[layer, pl.ds(dp, 1)][0]
+        with stage(f"L{layer}_wait_sq"):
+            await_bytes(sq_in.at[layer], q_recv.at[layer])
+        own_squares = sq[pl.ds(layer * dpn + dp, 1)][0]
         for o in range(1, dpn):
             own_squares = own_squares + sq_in[layer, o - 1]
-        row_scale = lax.rsqrt(own_squares[:, :1] / D + norm_eps)
-
-        def project(j):
-            for copy in part_copies[j]:
-                copy.wait_recv()
-            sent.extend(part_copies[j])
-            summed = part[layer, j, pl.ds(dp, 1)][0].astype(jnp.float32)
+        row_scale = lax.rsqrt(jnp.sum(own_squares, axis=1, keepdims=True) / D + norm_eps)
+
+        def project(group):
+            await_bytes(part_in.at[layer * GROUPS + group], p_recv.at[layer * GROUPS + group])
+            summed = part[pl.ds((layer * GROUPS + group) * dpn + dp, 1)][0].astype(jnp.float32)
             for o in range(1, dpn):
-                summed = summed + part_in[layer, j, o - 1].astype(jnp.float32)
-            return (summed * row_scale).astype(jnp.bfloat16).astype(jnp.float32)
+                summed = summed + part_in[layer * GROUPS + group, o - 1].astype(jnp.float32)
+            summed = (summed * row_scale[None]).astype(jnp.bfloat16).astype(jnp.float32)
+            return [summed[i] for i in range(GROUP)]
 
         def rotated(rows_in, h):
             one = rows_in[:, h * DK : (h + 1) * DK]
             return one * cosine + pltpu.roll(one, half, 1) * sine
 
-        query = project(0)
-        queries = [rotated(query, h) for h in range(heads)]
-        tall = jnp.concatenate(queries, axis=0)
-        tall_row = lax.broadcasted_iota(jnp.int32, tall.shape, 0) % seqs
-        wide = jnp.concatenate([jnp.where(tall_row == s, tall, 0.0) for s in range(seqs)], axis=1)
-        read = jnp.dot(
-            wide.astype(jnp.bfloat16), state_t[layer], preferred_element_type=jnp.float32
-        )
-        key = project(1)
-        rotated_keys = [rotated(key, h) * DK ** (-0.5) for h in range(heads)]
-        value = project(2)
-        gate = project(3)
-        silu = gate / (1.0 + jnp.exp(-gate))
-        gains = head_in[layer : layer + 1, :].astype(jnp.float32)
-        outs = []
-        for h in range(heads):
-            at = slice(h * DK, (h + 1) * DK)
-            score = jnp.sum(queries[h] * rotated_keys[h], axis=1, keepdims=True)
-            readout = read[h * seqs : (h + 1) * seqs, at] + score * value[:, at]
-            mean = jnp.sum(readout, axis=1, keepdims=True) / DK
-            square = jnp.sum(readout * readout, axis=1, keepdims=True) / DK
-            grouped = (readout - mean) * lax.rsqrt(square - mean * mean + group_eps)
-            outs.append(silu[:, at] * grouped * gains[:, at])
-        gated[layer, pl.ds(dp, 1)] = jnp.concatenate(outs, axis=1).astype(jnp.bfloat16)[None]
-        gated_copies = [
-            send(
-                gated.at[layer, dp],
-                gated.at[layer, dp],
-                g_send.at[layer, o],
-                g_recv.at[layer, o],
-                (tp, dp_peers[o]),
+        with stage(f"L{layer}_proj0_read"):
+            query, key = project(0)
+            queries = [rotated(query, h) for h in range(heads)]
+            tall = jnp.concatenate(queries, axis=0)
+            tall_row = lax.broadcasted_iota(jnp.int32, tall.shape, 0) % seqs
+            wide = jnp.concatenate([jnp.where(tall_row == s, tall, 0.0) for s in range(seqs)], axis=1)
+            read = jnp.dot(
+                wide.astype(jnp.bfloat16), state_t[layer], preferred_element_type=jnp.float32
             )
-            for o in range(1, dpn)
-        ]
-        turned = jnp.transpose(value)
-
-        def advance(first, last):
-            for s in range(first, last):
+            rotated_keys = [rotated(key, h) * DK ** (-0.5) for h in range(heads)]
+            scores = [
+                jnp.sum(queries[h] * rotated_keys[h], axis=1, keepdims=True) for h in range(heads)
+            ]
+            gains = head_in[layer : layer + 1, :].astype(jnp.float32)
+        with stage(f"L{layer}_proj1_norm"):
+            value, gate = project(1)
+            silu = gate / (1.0 + jnp.exp(-gate))
+            outs = []
+            for h in range(heads):
+                at = slice(h * DK, (h + 1) * DK)
+                readout = read[h * seqs : (h + 1) * seqs, at] + scores[h] * value[:, at]
+                mean = jnp.sum(readout, axis=1, keepdims=True) / DK
+                square = jnp.sum(readout * readout, axis=1, keepdims=True) / DK
+                grouped = (readout - mean) * lax.rsqrt(square - mean * mean + group_eps)
+                outs.append(silu[:, at] * grouped * gains[:, at])
+            gated[pl.ds(layer * dpn + dp, 1)] = jnp.concatenate(outs, axis=1).astype(jnp.bfloat16)[None]
+            for o in reversed(range(1, dpn)):
+                send(
+                    gated.at[layer * dpn + dp],
+                    gated.at[layer * dpn + dp],
+                    3,
+                    g_recv.at[layer],
+                    (tp, dp_peers[o]),
+                )
+
+        def advance(first_seq, last_seq):
+            for s in range(first_seq, last_seq):
                 for h in range(heads):
                     at = slice(h * DK, (h + 1) * DK)
                     new_states[layer, s, at] = (
@@ -370,42 +378,47 @@
                         + turned[at, s : s + 1] * rotated_keys[h][s : s + 1]
                     )
 
-        advance(0, seqs // 4)
+        with stage(f"L{layer}_adv1"):
+            turned = jnp.transpose(value)
+            advance(0, seqs // 2)
         got_back[layer].wait()
-        for copy in gated_copies:
-            copy.wait_recv()
-        sent += gated_copies
-        every = gated[layer].reshape(dpn * seqs, columns)
-        product = jnp.dot(every, w_back[layer], preferred_element_type=jnp.float32)
-        branch[layer] = product.reshape(tpn, rows, features).astype(jnp.bfloat16)
-        branch_copies = [
-            send(
-                branch.at[layer, tp_peers[o]],
-                branch_in.at[layer, o - 1],
-                b_send.at[layer, o],
-                b_recv.at[layer, o],
-                (tp_peers[o], dp),
-            )
-            for o in range(1, tpn)
-        ]
-        advance(seqs // 4, seqs)
-        if layer + 1 < LAYERS:
-            turn_state(layer + 1)
-        added = branch[layer, pl.ds(tp, 1)][0].astype(jnp.float32)
+        with stage(f"L{layer}_wait_g"):
+            await_bytes(gated.at[pl.ds(layer * dpn, dpn - 1)], g_recv.at[layer])
+        with stage(f"L{layer}_outdot"):
+            every = gated[layer * dpn : (layer + 1) * dpn].reshape(dpn * seqs, columns)
+            product = jnp.dot(every, w_back[layer], preferred_element_type=jnp.float32)
+            branch[first : first + tpn] = product.reshape(tpn, rows, features).astype(jnp.bfloat16)
+            for o in tp_order:
+                send(
+                    branch.at[first + tp_peers[o]],
+                    branch_in.at[layer, o - 1],
+                    4,
+                    b_recv.at[layer],
+                    (tp_peers[o], dp),
+                )
+        with stage(f"L{layer}_adv2"):
+            advance(seqs // 2, seqs)
+            if layer + 1 < LAYERS:
+                turn_state(layer + 1)
+        with stage(f"L{layer}_wait_b"):
+            await_bytes(branch_in.at[layer], b_recv.at[layer])
+        added = branch[pl.ds(first + tp, 1)][0].astype(jnp.float32)
         for o in range(1, tpn):
-            branch_copies[o - 1].wait_recv()
             added = added + branch_in[layer, o - 1].astype(jnp.float32)
-        sent += branch_copies
         new_x = (x_own + added).astype(jnp.bfloat16)
         if layer + 1 < LAYERS:
             fresh[...] = new_x
-            gathered[layer + 1, pl.ds(tp, 1)] = new_x[None]
+            gathered[pl.ds(first + tpn + tp, 1)] = new_x[None]
             x_own = new_x.astype(jnp.float32)
-            x_copies = spread_x(layer + 1, fresh)
+            spread_x(layer + 1, fresh)
         else:
             hidden[...] = new_x
-    for copy in sent:
-        copy.wait_send()
+    with stage("wait_sent"):
+        await_bytes(gathered.at[pl.ds(0, LAYERS * (tpn - 1))], send_sem.at[0])
+        await_bytes(sq.at[pl.ds(0, LAYERS * (dpn - 1))], send_sem.at[1])
+        await_bytes(part.at[pl.ds(0, LAYERS * GROUPS * (dpn - 1))], send_sem.at[2])
+        await_bytes(gated.at[pl.ds(0, LAYERS * (dpn - 1))], send_sem.at[3])
+        await_bytes(branch.at[pl.ds(0, LAYERS * (tpn - 1))], send_sem.at[4])
 
 
 def deliver_kernel(hidden_in, states_in, hidden, states, sem):
@@ -414,11 +427,11 @@
     copies = [pltpu.make_async_copy(hidden_in, hidden, sem.at[0])]
     for piece in range(layers * pieces):
         at = (piece // pieces, pl.ds(piece % pieces * (seqs // pieces), seqs // pieces))
-        copies.append(pltpu.make_async_copy(states_in.at[at], states.at[at], sem.at[piece + 1]))
+        copies.append(pltpu.make_async_copy(states_in.at[at], states.at[at], sem.at[1]))
     for copy in copies:
         copy.start()
-    for copy in copies:
-        copy.wait()
+    copies[0].wait()
+    await_bytes(states, sem.at[1])
 
 
 def body(tokens, lengths, states, norm_gain, w_query, w_key, w_value, w_gate, head_gain, w_out):
@@ -450,26 +463,25 @@
             pltpu.VMEM((LAYERS, seqs * DK, columns), bf16),
             pltpu.VMEM((LAYERS, KINDS, features, columns), bf16),
             pltpu.VMEM((LAYERS, columns, features), bf16),
-            pltpu.VMEM((LAYERS, tpn, rows, features), bf16),
-            pltpu.VMEM((LAYERS, KINDS, dpn, seqs, columns), bf16),
-            pltpu.VMEM((LAYERS, KINDS, dpn - 1, seqs, columns), bf16),
-            pltpu.VMEM((LAYERS, dpn, seqs, DK), f32),
+            pltpu.VMEM((LAYERS * tpn, rows, features), bf16),
+            pltpu.VMEM((LAYERS * GROUPS * dpn, GROUP, seqs, columns), bf16),
+            pltpu.VMEM((LAYERS * GROUPS, dpn - 1, GROUP, seqs, columns), bf16),
+            pltpu.VMEM((LAYERS * dpn, seqs, DK), f32),
             pltpu.VMEM((LAYERS, dpn - 1, seqs, DK), f32),
-            pltpu.VMEM((LAYERS, dpn, seqs, columns), bf16),
-            pltpu.VMEM((LAYERS, tpn, rows, features), bf16),
+            pltpu.VMEM((LAYERS * dpn, seqs, columns), bf16),
+            pltpu.VMEM((LAYERS * tpn, rows, features), bf16),
             pltpu.VMEM((LAYERS, tpn - 1, rows, features), bf16),
             pltpu.VMEM((rows, features), bf16),
-            dma((LAYERS * (KINDS + 2) + 4,)),
-            dma((LAYERS, tpn)),
-            dma((LAYERS, tpn)),
-            dma((LAYERS, KINDS, dpn)),
-            dma((LAYERS, KINDS, dpn)),
-            dma((LAYERS, dpn)),
-            dma((LAYERS, dpn)),
-            dma((LAYERS, dpn)),
-            dma((LAYERS, dpn)),
-            dma((LAYERS, tpn)),
-            dma((LAYERS, tpn)),
+            dma((4,)),
+            dma((LAYERS,)),
+            dma((LAYERS,)),
+            dma((LAYERS,)),
+            dma((5,)),
+            dma((LAYERS,)),
+            dma((LAYERS * GROUPS,)),
+            dma((LAYERS,)),
+            dma((LAYERS,)),
+            dma((LAYERS,)),
         ],
         compiler_params=pltpu.CompilerParams(collective_id=0, has_side_effects=True, vmem_limit_bytes=40 * 1024 * 1024),
     )(
@@ -497,7 +509,7 @@
         ),
         in_specs=[vmem, vmem],
         out_specs=(away, away),
-        scratch_shapes=[dma((LAYERS * OUT_PIECES + 1,))],
+        scratch_shapes=[dma((2,))],
         compiler_params=pltpu.CompilerParams(vmem_limit_bytes=8 * 1024 * 1024),
     )(hidden, new_states)
 

time: 43.1 us -> 41.1 us (0.954)
  Pallas kernels: 42.3 us -> 40.2 us
    pallas_call x1, Pallas kernels: 40.2 us -> 38.2 us  [body(): pl.pallas_call(step_kernel, out_shape=(pltpu.VMEM((rows, features), bf16)...]
where the time goes in v1:
time: 41.1 us; the launch traced here: 40.8 us
  Pallas kernels  40.2 us (98%)
  between operations  0.64 us (2%)
    pallas_call x1, Pallas kernels, body(): pl.pallas_call(step_kernel, out_shape=(pltpu.VMEM((rows, features), bf16)...  38.2 us
    pallas_call x1, Pallas kernels, body(): pl.pallas_call(deliver_kernel, out_shape=(jax.ShapeDtypeStruct((rows, fea...  2.02 us

profile of v1, /device:TPU:0, one launch (start us, length us, event | category | flops | bytes accessed | tf_op | source)
XLA Modules:
  0.0 40.8 jit_solution(7667114383079003759)
XLA Ops:
  0.6 38.2 %shard_map.113 = (bf16[8,1024]{1,0:T(8,128)(2,1)S(1)}, f32[2,16,256,128]{3,2,1,0:T(8,128)S(1)}) custom-call(bf16[8,1024]{1,0:T(8,128)(2,1)} %tokens.1, s32[16]{0:T(128)} %lengths.1, bf16[2,1024]{1,0:T(2,128)(2,1)} %norm_gain.1, bf16[2,256]{1,0:T(2,128)(2,1)} %head_gain.1, f32[2,16,256,128]{3,2,1,0:T(8,128)} %states.1, bf16[2,1024,256]{2,1,0:T(8,128)(2,1)} %w_query.1, ...), custom_call_target="tpu_custom_call" | custom-call | tf_op jit(solution)/shard_map/pallas_call | solution.py:450
  38.8 2.0 %shard_map.114 = (bf16[8,1024]{1,0:T(8,128)(2,1)}, f32[2,16,256,128]{3,2,1,0:T(8,128)}) custom-call(bf16[8,1024]{1,0:T(8,128)(2,1)S(1)} %get-tuple-element.4.hidden_in, f32[2,16,256,128]{3,2,1,0:T(8,128)S(1)} %get-tuple-element.5.states_in), custom_call_target="tpu_custom_call" | custom-call | tf_op jit(solution)/shard_map/pallas_call | solution.py:504

commit v2 on v1

--- a/solution.py
+++ b/solution.py
@@ -1,4 +1,5 @@
 import contextlib
+import functools
 import math
 
 import jax
@@ -206,6 +207,7 @@
     seqs, columns = new_states.shape[1:3]
     heads = columns // DK
     total = rows * tpn
+    per_block = seqs // rows
 
     barrier = pltpu.get_barrier_semaphore()
     tp_peers, dp_peers = peers_of(tp, tpn), peers_of(dp, dpn)
@@ -265,6 +267,9 @@
 
     tp_order = sorted(range(1, tpn), key=lambda o: (-o.bit_count(), -o))
 
+    dp_order = list(range(1, dpn))[::-1]
+    last_order = sorted(dp_order, key=lambda o: (o % 2, -o))
+
     def spread_x(layer, src):
         for o in tp_order:
             send(src, gathered.at[layer * tpn + tp], 0, x_recv.at[layer], (tp_peers[o], dp))
@@ -284,21 +289,8 @@
         await_bytes(w_in.at[layer], w_sem.at[layer])
         with stage(f"L{layer}_wait_x"):
             await_bytes(gathered.at[pl.ds(first, tpn - 1)], x_recv.at[layer])
-        with stage(f"L{layer}_sq"):
-            x_all = gathered[first : first + tpn].astype(jnp.float32).reshape(total, features)
-            squares = x_all[:, :DK] * x_all[:, :DK]
-            for at in range(DK, features, DK):
-                squares = squares + x_all[:, at : at + DK] * x_all[:, at : at + DK]
-            sq[layer * dpn : (layer + 1) * dpn] = squares.reshape(dpn, seqs, DK)
-            for o in reversed(range(1, dpn)):
-                send(
-                    sq.at[layer * dpn + dp_peers[o]],
-                    sq_in.at[layer, o - 1],
-                    1,
-                    q_recv.at[layer],
-                    (tp, dp_peers[o]),
-                )
-            normed = (x_all * norm_in[layer : layer + 1, :].astype(jnp.float32)).astype(jnp.bfloat16)
+        x_all = gathered[first : first + tpn].astype(jnp.float32).reshape(total, features)
+        normed = (x_all * norm_in[layer : layer + 1, :].astype(jnp.float32)).astype(jnp.bfloat16)
         for group in range(GROUPS):
             slot = (layer * GROUPS + group) * dpn
             with stage(f"L{layer}_dots{group}"):
@@ -307,7 +299,16 @@
                         normed, w_in[layer, group * GROUP + i], preferred_element_type=jnp.float32
                     )
                     part[slot : slot + dpn, i] = product.astype(jnp.bfloat16).reshape(dpn, seqs, columns)
-                for o in reversed(range(1, dpn)):
+                if group == 0:
+                    squares = x_all[:, :DK] * x_all[:, :DK]
+                    for at in range(DK, features, DK):
+                        squares = squares + x_all[:, at : at + DK] * x_all[:, at : at + DK]
+                    squares = jnp.concatenate([squares] * (sq.shape[2] // total), axis=0)
+                    sq[layer] = jnp.sum(jnp.transpose(squares), axis=0, keepdims=True)
+                if group == 0:
+                    for o in dp_order:
+                        send(sq.at[layer], sq_in.at[layer, o - 1], 1, q_recv.at[layer], (tp, dp_peers[o]))
+                for o in dp_order:
                     send(
                         part.at[slot + dp_peers[o]],
                         part_in.at[layer * GROUPS + group, o - 1],
@@ -317,10 +318,13 @@
                     )
         with stage(f"L{layer}_wait_sq"):
             await_bytes(sq_in.at[layer], q_recv.at[layer])
-        own_squares = sq[pl.ds(layer * dpn + dp, 1)][0]
+        all_squares = sq[layer]
         for o in range(1, dpn):
-            own_squares = own_squares + sq_in[layer, o - 1]
-        row_scale = lax.rsqrt(jnp.sum(own_squares, axis=1, keepdims=True) / D + norm_eps)
+            all_squares = all_squares + sq_in[layer, o - 1]
+        own = lax.broadcasted_iota(jnp.int32, (seqs, sq.shape[2]), 1) - dp * seqs
+        own = own == lax.broadcasted_iota(jnp.int32, (seqs, sq.shape[2]), 0)
+        own_squares = jnp.sum(jnp.where(own, all_squares, 0.0), axis=1, keepdims=True)
+        row_scale = lax.rsqrt(own_squares / D + norm_eps)
 
         def project(group):
             await_bytes(part_in.at[layer * GROUPS + group], p_recv.at[layer * GROUPS + group])
@@ -359,8 +363,9 @@
                 square = jnp.sum(readout * readout, axis=1, keepdims=True) / DK
                 grouped = (readout - mean) * lax.rsqrt(square - mean * mean + group_eps)
                 outs.append(silu[:, at] * grouped * gains[:, at])
-            gated[pl.ds(layer * dpn + dp, 1)] = jnp.concatenate(outs, axis=1).astype(jnp.bfloat16)[None]
-            for o in reversed(range(1, dpn)):
+            own_rows = jnp.concatenate(outs, axis=1).astype(jnp.bfloat16)
+            gated[pl.ds(layer * dpn + dp, 1)] = own_rows[None]
+            for o in dp_order:
                 send(
                     gated.at[layer * dpn + dp],
                     gated.at[layer * dpn + dp],
@@ -378,33 +383,57 @@
                         + turned[at, s : s + 1] * rotated_keys[h][s : s + 1]
                     )
 
+        def send_row(owner):
+            send(
+                branch.at[first + owner],
+                branch_in.at[layer, tp],
+                4,
+                b_recv.at[layer],
+                (owner, dp),
+            )
+
+        def project_out(rows_in, blocks):
+            product = jnp.dot(rows_in, w_back[layer], preferred_element_type=jnp.float32)
+            product = product.astype(jnp.bfloat16).reshape(len(blocks), per_block, rows, features)
+            for i, block in enumerate(blocks):
+                branch[pl.ds(first + block * per_block, per_block)] = product[i]
+            for block in blocks:
+                for k in range(per_block):
+                    owner = block * per_block + lax.rem(tp + 1 + k, per_block)
+                    pl.when(owner != tp)(functools.partial(send_row, owner))
+
+        got_back[layer].wait()
+        if layer + 1 == LAYERS:
+            with stage(f"L{layer}_own_out"):
+                project_out(own_rows, [dp])
         with stage(f"L{layer}_adv1"):
             turned = jnp.transpose(value)
             advance(0, seqs // 2)
-        got_back[layer].wait()
         with stage(f"L{layer}_wait_g"):
             await_bytes(gated.at[pl.ds(layer * dpn, dpn - 1)], g_recv.at[layer])
         with stage(f"L{layer}_outdot"):
-            every = gated[layer * dpn : (layer + 1) * dpn].reshape(dpn * seqs, columns)
-            product = jnp.dot(every, w_back[layer], preferred_element_type=jnp.float32)
-            branch[first : first + tpn] = product.reshape(tpn, rows, features).astype(jnp.bfloat16)
-            for o in tp_order:
-                send(
-                    branch.at[first + tp_peers[o]],
-                    branch_in.at[layer, o - 1],
-                    4,
-                    b_recv.at[layer],
-                    (tp_peers[o], dp),
+            if layer + 1 < LAYERS:
+                every = gated[layer * dpn : (layer + 1) * dpn].reshape(total, columns)
+                product = jnp.dot(every, w_back[layer], preferred_element_type=jnp.float32)
+                branch[first : first + tpn] = product.reshape(tpn, rows, features).astype(jnp.bfloat16)
+                for o in tp_order:
+                    send_row(tp_peers[o])
+            else:
+                project_out(
+                    jnp.concatenate([gated[pl.ds(layer * dpn + dp_peers[o], 1)][0] for o in last_order], axis=0),
+                    [dp_peers[o] for o in last_order],
                 )
         with stage(f"L{layer}_adv2"):
             advance(seqs // 2, seqs)
-            if layer + 1 < LAYERS:
+        if layer + 1 < LAYERS:
+            with stage(f"L{layer}_turn"):
                 turn_state(layer + 1)
         with stage(f"L{layer}_wait_b"):
-            await_bytes(branch_in.at[layer], b_recv.at[layer])
-        added = branch[pl.ds(first + tp, 1)][0].astype(jnp.float32)
+            await_bytes(branch.at[pl.ds(0, tpn - 1)], b_recv.at[layer])
+        branch_in[layer, pl.ds(tp, 1)] = branch[pl.ds(first + tp, 1)]
+        added = branch_in[layer, 0].astype(jnp.float32)
         for o in range(1, tpn):
-            added = added + branch_in[layer, o - 1].astype(jnp.float32)
+            added = added + branch_in[layer, o].astype(jnp.float32)
         new_x = (x_own + added).astype(jnp.bfloat16)
         if layer + 1 < LAYERS:
             fresh[...] = new_x
@@ -415,7 +444,7 @@
             hidden[...] = new_x
     with stage("wait_sent"):
         await_bytes(gathered.at[pl.ds(0, LAYERS * (tpn - 1))], send_sem.at[0])
-        await_bytes(sq.at[pl.ds(0, LAYERS * (dpn - 1))], send_sem.at[1])
+        await_bytes(sq_in, send_sem.at[1])
         await_bytes(part.at[pl.ds(0, LAYERS * GROUPS * (dpn - 1))], send_sem.at[2])
         await_bytes(gated.at[pl.ds(0, LAYERS * (dpn - 1))], send_sem.at[3])
         await_bytes(branch.at[pl.ds(0, LAYERS * (tpn - 1))], send_sem.at[4])
@@ -447,6 +476,7 @@
     away = pl.BlockSpec(memory_space=pltpu.HBM)
     dma = pltpu.SemaphoreType.DMA
     bf16, f32 = jnp.bfloat16, jnp.float32
+    lanes = rows * tpn * max(DK // (rows * tpn), 1)
     hidden, new_states = pl.pallas_call(
         step_kernel,
         out_shape=(
@@ -466,11 +496,11 @@
             pltpu.VMEM((LAYERS * tpn, rows, features), bf16),
             pltpu.VMEM((LAYERS * GROUPS * dpn, GROUP, seqs, columns), bf16),
             pltpu.VMEM((LAYERS * GROUPS, dpn - 1, GROUP, seqs, columns), bf16),
-            pltpu.VMEM((LAYERS * dpn, seqs, DK), f32),
-            pltpu.VMEM((LAYERS, dpn - 1, seqs, DK), f32),
+            pltpu.VMEM((LAYERS, 1, lanes), f32),
+            pltpu.VMEM((LAYERS, dpn - 1, 1, lanes), f32),
             pltpu.VMEM((LAYERS * dpn, seqs, columns), bf16),
             pltpu.VMEM((LAYERS * tpn, rows, features), bf16),
-            pltpu.VMEM((LAYERS, tpn - 1, rows, features), bf16),
+            pltpu.VMEM((LAYERS, tpn, rows, features), bf16),
             pltpu.VMEM((rows, features), bf16),
             dma((4,)),
             dma((LAYERS,)),

time: 41.1 us -> 39.4 us (0.959)
  the two profiles are of different devices: /device:TPU:0 before, /device:TPU:3 now
where the time goes in v2:
time: 39.4 us; the launch traced here: 39.2 us
  Pallas kernels  38.6 us (98%)
  between operations  0.64 us (2%)
    pallas_call x1, Pallas kernels, body(): pl.pallas_call(step_kernel, out_shape=(pltpu.VMEM((rows, features), bf16)...  36.5 us
    pallas_call x1, Pallas kernels, body(): pl.pallas_call(deliver_kernel, out_shape=(jax.ShapeDtypeStruct((rows, fea...  2.02 us

profile of v2, /device:TPU:3, one launch (start us, length us, event | category | flops | bytes accessed | tf_op | source)
XLA Modules:
  0.0 39.2 jit_solution(15503292256777022478)
XLA Ops:
  0.6 36.5 %shard_map.113 = (bf16[8,1024]{1,0:T(8,128)(2,1)S(1)}, f32[2,16,256,128]{3,2,1,0:T(8,128)S(1)}) custom-call(bf16[8,1024]{1,0:T(8,128)(2,1)} %tokens.1, s32[16]{0:T(128)} %lengths.1, bf16[2,1024]{1,0:T(2,128)(2,1)} %norm_gain.1, bf16[2,256]{1,0:T(2,128)(2,1)} %head_gain.1, f32[2,16,256,128]{3,2,1,0:T(8,128)} %states.1, bf16[2,1024,256]{2,1,0:T(8,128)(2,1)} %w_query.1, ...), custom_call_target="tpu_custom_call" | custom-call | tf_op jit(solution)/shard_map/pallas_call | solution.py:480
  37.2 2.0 %shard_map.114 = (bf16[8,1024]{1,0:T(8,128)(2,1)}, f32[2,16,256,128]{3,2,1,0:T(8,128)}) custom-call(bf16[8,1024]{1,0:T(8,128)(2,1)S(1)} %get-tuple-element.4.hidden_in, f32[2,16,256,128]{3,2,1,0:T(8,128)S(1)} %get-tuple-element.5.states_in), custom_call_target="tpu_custom_call" | custom-call | tf_op jit(solution)/shard_map/pallas_call | solution.py:534

commit v3 on v2

--- a/solution.py
+++ b/solution.py
@@ -268,7 +268,10 @@
     tp_order = sorted(range(1, tpn), key=lambda o: (-o.bit_count(), -o))
 
     dp_order = list(range(1, dpn))[::-1]
-    last_order = sorted(dp_order, key=lambda o: (o % 2, -o))
+    late_blocks = [dp_peers[o] for o in dp_order]
+    if dpn & (dpn - 1) == 0 and dpn > 2:
+        late_blocks = [dp_peers[o] // 2 * 2 + k for o in range(2, dpn, 2) for k in range(2)]
+        late_blocks.append(dp_peers[1])
 
     def spread_x(layer, src):
         for o in tp_order:
@@ -419,10 +422,8 @@
                 for o in tp_order:
                     send_row(tp_peers[o])
             else:
-                project_out(
-                    jnp.concatenate([gated[pl.ds(layer * dpn + dp_peers[o], 1)][0] for o in last_order], axis=0),
-                    [dp_peers[o] for o in last_order],
-                )
+                late_rows = [gated[pl.ds(layer * dpn + block, 1)][0] for block in late_blocks]
+                project_out(jnp.concatenate(late_rows, axis=0), late_blocks)
         with stage(f"L{layer}_adv2"):
             advance(seqs // 2, seqs)
         if layer + 1 < LAYERS:

time: 39.4 us -> 39.2 us (level)
  the two profiles are of different devices: /device:TPU:3 before, /device:TPU:2 now
where the time goes in v3:
time: 39.2 us; the launch traced here: 38.9 us
  Pallas kernels  38.3 us (98%)
  between operations  0.64 us (2%)
    pallas_call x1, Pallas kernels, body(): pl.pallas_call(step_kernel, out_shape=(pltpu.VMEM((rows, features), bf16)...  36.3 us
    pallas_call x1, Pallas kernels, body(): pl.pallas_call(deliver_kernel, out_shape=(jax.ShapeDtypeStruct((rows, fea...  2.02 us

profile of v3, /device:TPU:2, one launch (start us, length us, event | category | flops | bytes accessed | tf_op | source)
XLA Modules:
  0.0 38.9 jit_solution(6318026415422505225)
XLA Ops:
  0.6 36.3 %shard_map.113 = (bf16[8,1024]{1,0:T(8,128)(2,1)S(1)}, f32[2,16,256,128]{3,2,1,0:T(8,128)S(1)}) custom-call(bf16[8,1024]{1,0:T(8,128)(2,1)} %tokens.1, s32[16]{0:T(128)} %lengths.1, bf16[2,1024]{1,0:T(2,128)(2,1)} %norm_gain.1, bf16[2,256]{1,0:T(2,128)(2,1)} %head_gain.1, f32[2,16,256,128]{3,2,1,0:T(8,128)} %states.1, bf16[2,1024,256]{2,1,0:T(8,128)(2,1)} %w_query.1, ...), custom_call_target="tpu_custom_call" | custom-call | tf_op jit(solution)/shard_map/pallas_call | solution.py:481
  36.9 2.0 %shard_map.114 = (bf16[8,1024]{1,0:T(8,128)(2,1)}, f32[2,16,256,128]{3,2,1,0:T(8,128)}) custom-call(bf16[8,1024]{1,0:T(8,128)(2,1)S(1)} %get-tuple-element.4.hidden_in, f32[2,16,256,128]{3,2,1,0:T(8,128)S(1)} %get-tuple-element.5.states_in), custom_call_target="tpu_custom_call" | custom-call | tf_op jit(solution)/shard_map/pallas_call | solution.py:535
